TPU v7x, 32 devices: a whole 2x2x4 slice. The times are simulated.
32 devices in a mesh: grp: 2 (over y), ep: 4 (over z), tp: 4 (over x, core).
Axes of the slice: x: 2, y: 2, z: 4, core: 2. Of those that a mesh axis runs over, the one named last changes fastest.
Arguments:
- tokens: bfloat16 [8, 2048], P(('grp', 'ep')), parts along dimension 0, may hold values from -6 to 6
- conv_state: bfloat16 [8, 3, 1024], P(('grp', 'ep'), None, 'tp'), parts along dimension 0, may hold values from -6 to 6
- state_h: float32 [8, 1024], P(('grp', 'ep'), 'tp'), parts along dimension 0, may hold values from -6 to 6
- mixer_gain: bfloat16 [2048], replicated, may hold values from 0.099609375 to 1.8984375
- expert_gain: bfloat16 [2048], replicated, may hold values from 0.099609375 to 1.8984375
- input_proj: bfloat16 [2048, 1024], P('ep', 'tp'), may hold values from -0.125 to 0.125
- branch_proj: bfloat16 [2048, 1024], P('ep', 'tp'), may hold values from -0.125 to 0.125
- conv_taps: bfloat16 [4, 1024], P(None, 'tp'), may hold values from -3 to 3
- write_map: bfloat16 [8, 128, 128], P('tp'), may hold values from -0.5 to 0.5
- decay_map: bfloat16 [8, 128, 128], P('tp'), may hold values from -0.5 to 0.5
- decay_rate: float32 [1024], P('tp'), may hold values from 0.01 to 0.4
- output_proj: bfloat16 [1024, 2048], P('tp'), may hold values from -0.1875 to 0.1875
- route_ids: int32 [8, 2], P('grp'), parts along dimension 0, may hold values from 0 to 3, all different within a row; in each aligned block of 4 rows (0 to 3, 4 to 7, ...) at most 4 rows name the same one
- route_scores: float32 [8, 2], P('grp'), parts along dimension 0, may hold values from 0.5 to 4
- expert_gate: bfloat16 [4, 2048, 1024], P('ep', None, 'tp'), may hold values from -0.125 to 0.125
- expert_up: bfloat16 [4, 2048, 1024], P('ep', None, 'tp'), may hold values from -0.125 to 0.125
- expert_down: bfloat16 [4, 1024, 2048], P('ep', 'tp'), may hold values from -0.1875 to 0.1875
- branch_gate: bfloat16 [2048], replicated, may hold values from -0.125 to 0.125
- shared_gate: bfloat16 [2048, 16384], P(None, ('ep', 'tp')), may hold values from -0.125 to 0.125
- shared_up: bfloat16 [2048, 16384], P(None, ('ep', 'tp')), may hold values from -0.125 to 0.125
- shared_down: bfloat16 [16384, 2048], P(('ep', 'tp')), may hold values from -0.0625 to 0.0625
Outputs:
- result: bfloat16 [8, 2048], P(('grp', 'ep'), 'tp'), parts along dimension 0
- state_next: float32 [8, 1024], P(('grp', 'ep'), 'tp'), parts along dimension 0
- conv_next: bfloat16 [8, 3, 1024], P(('grp', 'ep'), None, 'tp'), parts along dimension 0
There are 2 independent parts, one for each index of `grp`. A program takes and returns all parts, laid end to end along the dimension named above; an argument that names none is the same for every part. Nothing has to cross between parts.
Inputs may be any that keep to these rules, and one draw needn't show every extreme that they name: `route_ids`: the 2 experts of a token differ; no expert is named by more than 4 tokens, a bound that some block reaches.
All inputs are finite; a program needn't handle non-finite values.
Results may differ from a plain program's by a relative error of at most 0.013.
Values may be sent and summed in bfloat16 or wider, within the bound.
A program may use at most 64 MiB of HBM per device.

v0:
```python
import jax
import jax.numpy as jnp
from jax import lax
from jax.sharding import PartitionSpec as P


def rms_norm(array_in, gain_vec):
    values = array_in.astype(jnp.float32)
    scaled = values * lax.rsqrt(jnp.mean(values * values, axis=-1, keepdims=True) + 1e-06)
    return (scaled * gain_vec.astype(jnp.float32)).astype(jnp.bfloat16)


def on_device(
    tokens,
    conv_state,
    state_h,
    mixer_gain,
    expert_gain,
    input_proj,
    branch_proj,
    conv_taps,
    write_map,
    decay_map,
    decay_rate,
    output_proj,
    route_ids,
    route_scores,
    expert_gate,
    expert_up,
    expert_down,
    branch_gate,
    shared_gate,
    shared_up,
    shared_down,
):
    seq_rows = tokens.shape[0]
    channels = input_proj.shape[1]
    normed = rms_norm(tokens, mixer_gain)
    slices = lax.all_to_all(normed, "ep", split_axis=1, concat_axis=0, tiled=True)
    projected = lax.psum_scatter(
        jnp.concatenate(
            [
                jnp.dot(slices, input_proj, preferred_element_type=jnp.float32),
                jnp.dot(slices, branch_proj, preferred_element_type=jnp.float32),
            ],
            axis=1,
        ),
        "ep",
        scatter_dimension=0,
        tiled=True,
    )
    inner_x = projected[:, :channels].astype(jnp.bfloat16)
    branch_x = projected[:, channels:].astype(jnp.bfloat16)
    window_rows = jnp.concatenate([conv_state, inner_x[:, None, :]], axis=1)
    convolved = jnp.sum(
        window_rows.astype(jnp.float32) * conv_taps.astype(jnp.float32)[None], axis=1
    )
    head_count = write_map.shape[0]
    head_width = write_map.shape[1]
    conv_round = convolved.astype(jnp.bfloat16).reshape(seq_rows, head_count, head_width)
    write_gate = jax.nn.sigmoid(
        jnp.einsum(
            "shi,hij->shj", conv_round, write_map, preferred_element_type=jnp.float32
        ).reshape(seq_rows, channels)
    )
    decay_gate = jax.nn.sigmoid(
        jnp.einsum(
            "shi,hij->shj", conv_round, decay_map, preferred_element_type=jnp.float32
        ).reshape(seq_rows, channels)
    )
    log_keep = -8.0 * decay_gate * decay_rate
    state_next = (
        jnp.exp(log_keep) * state_h + jnp.sqrt(-jnp.expm1(2.0 * log_keep)) * write_gate * convolved
    )
    mixed = (state_next * jax.nn.gelu(branch_x.astype(jnp.float32))).astype(jnp.bfloat16)
    mixed_out = lax.psum(jnp.dot(mixed, output_proj, preferred_element_type=jnp.float32), "tp")
    resid = (tokens.astype(jnp.float32) + mixed_out).astype(jnp.bfloat16)
    normed2 = rms_norm(resid, expert_gain)
    gathered = lax.all_gather(normed2, "ep", axis=0, tiled=True)
    all_rows = route_ids.shape[0]
    top_count = route_ids.shape[1]
    ep_count = lax.axis_size("ep")
    capacity = 2 * top_count * all_rows // ep_count
    expert = lax.axis_index("ep")
    flat_ids = route_ids.reshape(-1)
    is_mine = (flat_ids == expert).astype(jnp.int32)
    slot_index = jnp.cumsum(is_mine) - 1
    pick_table = (
        (slot_index[None, :] == jnp.arange(capacity, dtype=jnp.int32)[:, None])
        & (is_mine[None, :] == 1)
    ).astype(jnp.float32)
    route_weight = route_scores / jnp.sum(route_scores, axis=1, keepdims=True)
    slot_weight = jnp.dot(pick_table, route_weight.reshape(-1), precision=lax.Precision.HIGHEST)
    chosen = jnp.sum(pick_table.reshape(capacity, all_rows, top_count), axis=2)
    picked = jnp.dot(
        chosen.astype(jnp.bfloat16), gathered, preferred_element_type=jnp.float32
    ).astype(jnp.bfloat16)
    gate_pre = jnp.dot(picked, expert_gate[0], preferred_element_type=jnp.float32)
    up_pre = jnp.dot(picked, expert_up[0], preferred_element_type=jnp.float32)
    hidden = (jax.nn.silu(gate_pre) * up_pre).astype(jnp.bfloat16)
    expert_out = jnp.dot(hidden, expert_down[0], preferred_element_type=jnp.float32)
    expert_part = jnp.dot(
        chosen.T, slot_weight[:, None] * expert_out, precision=lax.Precision.HIGHEST
    )
    dense_hidden = (
        jax.nn.silu(jnp.dot(gathered, shared_gate, preferred_element_type=jnp.float32))
        * jnp.dot(gathered, shared_up, preferred_element_type=jnp.float32)
    ).astype(jnp.bfloat16)
    branch_mix = jax.nn.sigmoid(jnp.dot(gathered, branch_gate, preferred_element_type=jnp.float32))
    dense_out = jnp.dot(dense_hidden, shared_down, preferred_element_type=jnp.float32)
    partials = expert_part + branch_mix[:, None] * dense_out
    tp_count = lax.axis_size("tp")
    col_width = partials.shape[1] // tp_count
    feature_part = lax.psum_scatter(partials, "tp", scatter_dimension=1, tiled=True)
    summed = lax.psum_scatter(feature_part, "ep", scatter_dimension=0, tiled=True)
    own_cols = lax.dynamic_slice_in_dim(resid, lax.axis_index("tp") * col_width, col_width, 1)
    result = (own_cols.astype(jnp.float32) + summed).astype(jnp.bfloat16)
    conv_next = window_rows[:, 1:]
    return (result, state_next, conv_next)


def solution(mesh):
    placed = (
        P(("grp", "ep"), None),
        P(("grp", "ep"), None, "tp"),
        P(("grp", "ep"), "tp"),
        P(),
        P(),
        P("ep", "tp"),
        P("ep", "tp"),
        P(None, "tp"),
        P("tp", None, None),
        P("tp", None, None),
        P("tp"),
        P("tp", None),
        P("grp", None),
        P("grp", None),
        P("ep", None, "tp"),
        P("ep", None, "tp"),
        P("ep", "tp", None),
        P(),
        P(None, ("ep", "tp")),
        P(None, ("ep", "tp")),
        P(("ep", "tp"), None),
    )
    return jax.shard_map(
        on_device,
        mesh=mesh,
        in_specs=placed,
        out_specs=(P(("grp", "ep"), "tp"), P(("grp", "ep"), "tp"), P(("grp", "ep"), None, "tp")),
        check_vma=False,
    )
```

profile of v0, /device:TPU:0, one launch (start us, length us, event | category | flops | bytes accessed | tf_op | source)
XLA Modules:
  0.0 123.7 jit_solution(2191744457980489492)
XLA Ops:
  7.2 0.0 copy-start
  7.2 0.8 broadcast_in_dim.30
  8.0 1.3 %multiply_reduce_fusion.1 = f32[]{:T(128)} fusion(bf16[1,2048]{1,0:T(2,128)(2,1)} %param.21), kind=kLoop, calls=%fused_computation.29 | loop fusion | flops 6143 | bytes 4100 | tf_op jit(solution)/shard_map/reduce_sum | solution.py:9
  10.0 0.7 multiply_convert_fusion
  10.7 0.5 broadcast.102
  11.2 0.7 reduce.8
  11.9 0.6 reshape.185
  12.5 6.3 %all-to-all-start = ((bf16[4,2,256]{2,1,0:T(2,128)(2,1)}), bf16[4,2,256]{2,1,0:T(2,128)(2,1)S(1)}, u32[]{:S(2)}, u32[]{:S(2)}) async-start(bf16[4,2,256]{2,1,0:T(2,128)(2,1)} %reshape.185), calls=%async_computation | async-start | bytes 8192 | tf_op jit(solution)/shard_map/all_to_all | solution.py:39
  18.8 0.0 reduce-scatter.4.cloned.1.call-start
  18.8 0.7 broadcast_compare_fusion
  19.5 0.1 copy.40
  19.6 0.1 reshape.159
  19.7 0.2 reduce-window_clone.1
  19.9 0.1 sub.8
  20.0 0.1 copy.41
  20.1 0.1 copy.42
  20.2 0.1 eq.62
  20.3 0.7 reduce_sum.48
  21.0 0.7 broadcast_divide_fusion
  21.7 0.1 copy.43
  21.8 0.1 reshape.168
  21.9 0.1 convolution_bitcast_fusion
  22.0 0.7 broadcast_in_dim.31
  22.7 0.7 reshape.170
  23.4 1.3 %dynamic-slice = u32[1]{0:T(128)} dynamic-slice(u32[32]{0:T(128)} %constant.60, u32[]{:T(128)S(6)} %add.81), dynamic_slice_sizes={1} | dynamic-slice | bytes 12
  24.6 0.0 all-to-all-done
  24.7 1.1 fusion.16
  25.8 1.1 fusion.18
  26.9 12.3 %all-reduce = bf16[4,512]{1,0:T(4,128)(2,1)S(1)} all-reduce(f32[4,512]{1,0:T(4,128)S(1)} %pad_maximum_fusion), channel_id=2, replica_groups=mesh['grp'=2,'ep'=4,'tp'=4] {'ep'}, use_global_device_ids=true, to_apply=%region_1.0.clone | all-reduce | flops 2048 | bytes 12288
  39.2 0.6 dynamic-slice_convert_fusion
  39.9 0.7 multiply_reduce_fusion.2
  40.6 1.0 fusion.48
  41.5 1.0 fusion.46
  42.5 0.7 fusion.60
  43.2 0.7 multiply_add_fusion
  43.9 0.0 copy-start.2
  43.9 1.5 %fusion.38 = f32[1,2048]{1,0:T(1,128)S(1)} fusion(bf16[256,2048]{1,0:T(8,128)(2,1)} %param.32, f32[1,256]{1,0:T(1,128)S(1)} %multiply_add_fusion, bf16[1,512]{1,0:T(2,128)(2,1)S(1)} %dynamic-slice_convert_fusion), kind=kOutput, calls=%fused_computation.62 | convolution fusion | flops 1051392 | bytes 1058816 | tf_op jit(solution)/shard_map/dot_general | solution.py:76
  45.4 5.7 %psum.7 = f32[1,2048]{1,0:T(1,128)S(1)} all-reduce(f32[1,2048]{1,0:T(1,128)S(1)} %fusion.38), channel_id=1, replica_groups=mesh['grp'=2,'ep'=4,'tp'=4] {'tp'}, use_global_device_ids=true, to_apply=%region_3.0 | all-reduce | flops 2048 | bytes 16384 | tf_op jit(solution)/shard_map/psum | solution.py:76
  51.2 1.3 %multiply_reduce_fusion = (f32[]{:T(128)}, bf16[1,2048]{1,0:T(2,128)(2,1)S(1)}) fusion(f32[1,2048]{1,0:T(1,128)S(1)} %psum.7, bf16[1,2048]{1,0:T(2,128)(2,1)} %param.21), kind=kLoop, calls=%fused_computation.26 | loop fusion | flops 12287 | bytes 16388 | tf_op jit(solution)/shard_map/reduce_sum | solution.py:9
  53.2 13.1 %all-gather = bf16[4,1,2048]{2,1,0:T(2,128)(2,1)S(1)} all-gather(bf16[1,1,2048]{2,1,0:T(2,128)(2,1)S(1)} %convert_bitcast_fusion), channel_id=1, replica_groups=mesh['grp'=2,'ep'=4,'tp'=4] {'ep'}, dimensions={0}, use_global_device_ids=true | all-gather | bytes 20480 | tf_op jit(solution)/shard_map/all_gather | solution.py:79
  66.4 0.1 convolution_convert_fusion
  66.5 1.5 %fusion.10 = f32[4,256]{1,0:T(4,128)S(1)} fusion(bf16[4,2048]{1,0:T(4,128)(2,1)S(1)} %convolution_convert_fusion, bf16[1,2048,256]{2,1,0:T(8,128)(2,1)} %param.35), kind=kOutput, calls=%fused_computation.16 | convolution fusion | flops 4194304 | bytes 1069056 | tf_op jit(solution)/shard_map/dot_general | solution.py:98
  67.9 0.0 copy-done
  68.0 2.0 %convolution_multiply_fusion.1 = f32[4,2048]{1,0:T(4,128)S(1)} fusion(bf16[4,2048]{1,0:T(4,128)(2,1)S(1)} %convolution_convert_fusion, bf16[1,256,2048]{2,1,0:T(8,128)(2,1)S(1)} %copy-done, bf16[1,2048,256]{2,1,0:T(8,128)(2,1)} %param.36, f32[4]{0:T(128)S(1)} %convolution_bitcast_fusion, f32[4,256]{1,0:T(4,128)S(1)} %fusion.10), kind=kOutput, calls=%fused_computation.2 | convolution fusion | flops 8402944 | bytes 2150416 | tf_op jit(solution)/shard_map/dot_general | solution.py:101
  69.9 0.3 fusion.61
  70.2 2.8 %fusion.62 = f32[4,1024]{1,0:T(4,128)S(1)} fusion(bf16[4,2048]{1,0:T(4,128)(2,1)S(1)} %bitcast.86, bf16[2048,1024]{1,0:T(8,128)(2,1)} %param.39), kind=kOutput, calls=%fused_computation.94 | convolution fusion | flops 16777216 | bytes 4227072 | tf_op jit(solution)/shard_map/dot_general | solution.py:106
  73.0 0.0 copy-done.2
  73.0 0.1 fusion.6
  73.2 0.0 copy-start.1
  73.2 4.7 %fusion = f32[4,2048]{1,0:T(4,128)S(1)} fusion(f32[4,2048]{1,0:T(4,128)S(1)} %fusion.61, bf16[1024,2048]{1,0:T(8,128)(2,1)} %param.41, bf16[4,2048]{1,0:T(4,128)(2,1)S(1)} %bitcast.88, bf16[2048,1024]{1,0:T(8,128)(2,1)} %param.40, f32[4,1024]{1,0:T(4,128)S(1)} %fusion.62, f32[4]{0:T(128)S(1)} %fusion.6), kind=kOutput, calls=%fused_computation.1 | convolution fusion | flops 33595392 | bytes 8486928 | tf_op jit(solution)/shard_map/dot_general | solution.py:110
  77.9 1.4 %copy.47 = f32[4,2048]{0,1:T(8,128)} copy(f32[4,2048]{1,0:T(4,128)S(1)} %fusion) | data formatting | bytes 65536
  79.2 0.0 reduce-scatter.4.cloned.1.call-update
  79.3 0.0 copy-done.1
  79.3 0.6 pad_maximum_fusion.1
  79.9 22.8 %reduce-scatter.4.cloned.1.call-done = f32[512,4]{1,0:T(8,128)} async-done(((f32[2048,4]{1,0:T(8,128)}), f32[512,4]{1,0:T(8,128)}) %reduce-scatter.4.cloned.1.call-update) | async-done | bytes 8208
  102.7 1.1 copy.48
  103.7 11.9 %all-reduce.1 = f32[4,512]{1,0:T(4,128)S(1)} all-reduce(f32[4,512]{1,0:T(4,128)S(1)} %copy.48), channel_id=4, replica_groups=mesh['grp'=2,'ep'=4,'tp'=4] {'ep'}, use_global_device_ids=true, to_apply=%region_9.10.clone | all-reduce | flops 2048 | bytes 16384
  115.6 1.2 fusion.24
  (9 shorter events, 0.1 us)
Async XLA Ops:
  7.2 60.8 %copy-start = (bf16[1,256,2048]{2,1,0:T(8,128)(2,1)S(1)}, bf16[1,256,2048]{2,1,0:T(8,128)(2,1)}, u32[]{:S(2)}) copy-start(bf16[1,256,2048]{2,1,0:T(8,128)(2,1)} %param.37) | copy-start | bytes 3145732
  12.5 12.2 %all-to-all-start = ((bf16[4,2,256]{2,1,0:T(2,128)(2,1)}), bf16[4,2,256]{2,1,0:T(2,128)(2,1)S(1)}, u32[]{:S(2)}, u32[]{:S(2)}) async-start(bf16[4,2,256]{2,1,0:T(2,128)(2,1)} %reshape.185), calls=%async_computation | async-start | bytes 8192 | tf_op jit(solution)/shard_map/all_to_all | solution.py:39
  18.8 83.8 %reduce-scatter.4.cloned.1.call-start = ((), (), s32[]{:S(2)}) async-start(), calls=%async_computation.2 | async-start | bytes 1310720
  43.9 29.1 %copy-start.2 = (f32[1,256]{1,0:T(1,128)}, f32[1,256]{1,0:T(1,128)S(1)}, u32[]{:S(2)}) copy-start(f32[1,256]{1,0:T(1,128)S(1)} %multiply_add_fusion) | copy-start | bytes 3076
  73.2 6.1 %copy-start.1 = (bf16[1,3,256]{2,1,0:T(4,128)(2,1)S(1)}, bf16[1,3,256]{2,1,0:T(4,128)(2,1)}, u32[]{:S(2)}) copy-start(bf16[1,3,256]{2,1,0:T(4,128)(2,1)} %param.22) | copy-start | bytes 4612
Sparse Core Ops, SparseCore 0:
  79.4 23.2 reduce-scatter.3
where the time goes:
time: 125 us; the launch traced here: 124 us
  blocking collectives  43.1 us (34%)
  waiting for transfers between devices  22.8 us (18%)
  matrix products  17.2 us (14%)
  between operations  15.5 us (12%)
  other arithmetic  11.8 us (9%)
  local copies, waits for them, and re-layouts  6.92 us (6%)
  starting transfers between devices  6.35 us (5%)
    unnamed x2, blocking collectives  24.2 us
    unnamed x2, waiting for transfers between devices  22.8 us
    all_gather x1, blocking collectives, on_device(): gathered = lax.all_gather(normed2, 'ep', axis=0, tiled=True)  13.1 us
    all_to_all x1, starting transfers between devices, on_device(): lax.all_to_all(normed, 'ep', split_axis=1, concat_axis=0, tiled=True)  6.35 us
    psum x1, blocking collectives, on_device(): lax.psum(jnp.dot(mixed, output_proj, preferred_element_type=jnp.float32),...  5.74 us
    unnamed x14, local copies, waits for them, and re-layouts  5.55 us
    dot_general x1, matrix products, on_device(): jnp.dot(dense_hidden, shared_down, preferred_element_type=jnp.float32)  4.7 us
    dot_general x1, matrix products, on_device(): jnp.dot(gathered, shared_gate, preferred_element_type=jnp.float32)  2.84 us
  transfers between devices with their start and end apart: 2, of which 1 were waited for; matrix products, arithmetic and copies ran while one was open for 5% of the time, Pallas kernels for 0%

commit v1 on v0

v1 whole, which is shorter than its diff:
```python
import functools

import jax
import jax.numpy as jnp
from jax import lax
from jax.experimental import pallas as pl
from jax.experimental.pallas import tpu as pltpu
from jax.sharding import PartitionSpec as P

MESH = pl.DeviceIdType.MESH
F32 = jnp.float32
BF16 = jnp.bfloat16


def each(count, step):
    if count <= 16:
        for number in range(count):
            step(number)
    else:

        def body(number, carry):
            step(number)
            return carry

        lax.fori_loop(0, count, body, 0)


def mm(left, right):
    return jnp.dot(left, right, preferred_element_type=F32)


def silu(value):
    return value * jax.nn.sigmoid(value)


def layer_kernel(
    ep,
    tp,
    tokens,
    conv_state,
    state_h,
    mixer_gain,
    expert_gain,
    input_proj,
    branch_proj,
    conv_taps,
    write_map,
    decay_map,
    decay_rate,
    output_proj,
    route_ids,
    route_scores,
    expert_gate,
    expert_up,
    expert_down,
    branch_gate,
    shared_gate,
    shared_up,
    shared_down,
    result_out,
    state_out,
    conv_out,
    tok_all,
    conv_all,
    state_all,
    mgain,
    egain,
    iproj,
    bproj,
    taps,
    wmap,
    dmap,
    rate,
    oproj,
    ids,
    scores,
    eg_w,
    eu_w,
    ed_w,
    bgate,
    sg_w,
    su_w,
    sd_w,
    norm_s,
    part_in,
    part_out,
    part_send,
    part_recv,
    resid_s,
    next_s,
    inner_s,
    local_sem,
    tok_ss,
    tok_rs,
    conv_ss,
    conv_rs,
    state_ss,
    state_rs,
    in_ss,
    in_rs,
    out_ss,
    out_rs,
    last_ss,
    last_rs,
):
    me_e = lax.axis_index("ep")
    me_t = lax.axis_index("tp")
    rows = ep
    width = tok_all.shape[-1]
    channels = iproj.shape[1]
    depth = iproj.shape[0]
    col_width = part_send.shape[-1]
    me_flat = me_e * tp + me_t

    small = [
        (tokens, tok_all.at[me_e]),
        (conv_state.at[0], conv_all.at[me_e]),
        (state_h, state_all.at[me_e]),
        (mixer_gain, mgain),
        (input_proj, iproj),
        (branch_proj, bproj),
        (conv_taps, taps),
        (write_map, wmap),
        (decay_map, dmap),
        (decay_rate, rate),
        (output_proj, oproj),
        (expert_gain, egain),
        (route_ids, ids),
        (route_scores, scores),
        (branch_gate, bgate),
    ]
    large = [
        (shared_gate, sg_w),
        (shared_up, su_w),
        (expert_gate.at[0], eg_w),
        (expert_up.at[0], eu_w),
        (expert_down.at[0], ed_w),
        (shared_down, sd_w),
    ]
    local = [
        pltpu.make_async_copy(src, dst, local_sem.at[number])
        for number, (src, dst) in enumerate(small + large)
    ]
    (
        c_tok,
        c_conv,
        c_state,
        c_mgain,
        c_iproj,
        c_bproj,
        c_taps,
        c_wmap,
        c_dmap,
        c_rate,
        c_oproj,
        c_egain,
        c_ids,
        c_scores,
        c_bgate,
        c_sg,
        c_su,
        c_eg,
        c_eu,
        c_ed,
        c_sd,
    ) = local
    for copy in local[: len(small)]:
        copy.start()

    barrier = pltpu.get_barrier_semaphore()

    def greet(number):
        flat = lax.rem(me_flat + 1 + number, ep * tp)
        pl.semaphore_signal(
            barrier,
            inc=1,
            device_id={"ep": flat // tp, "tp": lax.rem(flat, tp)},
            device_id_type=MESH,
        )

    each(ep * tp - 1, greet)
    pl.semaphore_wait(barrier, ep * tp - 1)

    def over_ep(buf, ssem, rsem, slot, peer):
        return pltpu.make_async_remote_copy(
            src_ref=buf.at[slot],
            dst_ref=buf.at[slot],
            send_sem=ssem.at[peer],
            recv_sem=rsem.at[slot],
            device_id={"ep": peer},
            device_id_type=MESH,
        )

    def over_tp(buf, ssem, rsem, slot, peer):
        return pltpu.make_async_remote_copy(
            src_ref=buf.at[slot],
            dst_ref=buf.at[slot],
            send_sem=ssem.at[peer],
            recv_sem=rsem.at[slot],
            device_id={"tp": peer},
            device_id_type=MESH,
        )

    def ep_peer(number):
        return lax.rem(me_e + 1 + number, ep)

    def tp_peer(number):
        return lax.rem(me_t + 1 + number, tp)

    def send_ep(buf, ssem, rsem):
        each(ep - 1, lambda n: over_ep(buf, ssem, rsem, me_e, ep_peer(n)).start())

    def recv_ep(buf, ssem, rsem):
        each(ep - 1, lambda n: over_ep(buf, ssem, rsem, ep_peer(n), ep_peer(n)).wait_recv())

    def sent_ep(buf, ssem, rsem):
        each(ep - 1, lambda n: over_ep(buf, ssem, rsem, me_e, ep_peer(n)).wait_send())

    c_tok.wait()
    send_ep(tok_all, tok_ss, tok_rs)
    c_conv.wait()
    send_ep(conv_all, conv_ss, conv_rs)
    c_state.wait()
    send_ep(state_all, state_ss, state_rs)
    for copy in local[len(small) :]:
        copy.start()

    c_mgain.wait()
    c_iproj.wait()
    c_bproj.wait()
    recv_ep(tok_all, tok_ss, tok_rs)
    tok = jnp.concatenate([tok_all[row].astype(F32) for row in range(rows)], axis=0)
    scale = lax.rsqrt(jnp.mean(tok * tok, axis=-1, keepdims=True) + 1e-06)
    normed = tok * scale * mgain[...].astype(F32).reshape(1, width)
    if depth % 128 == 0:
        norm_s[...] = normed
        mine = norm_s[:, pl.ds(pl.multiple_of(me_e * depth, depth), depth)]
    else:
        mine = pltpu.roll(normed, lax.rem(width - me_e * depth, width), 1)[:, :depth]
    mine = mine.astype(BF16)
    part_in[me_e] = jnp.concatenate([mm(mine, iproj[...]), mm(mine, bproj[...])], axis=1).astype(
        BF16
    )
    send_ep(part_in, in_ss, in_rs)

    c_taps.wait()
    c_wmap.wait()
    c_dmap.wait()
    c_rate.wait()
    c_oproj.wait()
    recv_ep(conv_all, conv_ss, conv_rs)
    recv_ep(state_all, state_ss, state_rs)
    tap = taps[...].astype(F32)
    past = tap.shape[0] - 1
    history = jnp.concatenate(
        [
            jnp.sum(conv_all[row].astype(F32) * tap[:past], axis=0, keepdims=True)
            for row in range(rows)
        ],
        axis=0,
    )
    state = jnp.concatenate([state_all[row] for row in range(rows)], axis=0)
    rates = rate[...].reshape(1, channels)

    recv_ep(part_in, in_ss, in_rs)
    projected = jnp.sum(part_in[...].astype(F32), axis=0)
    inner_x = projected[:, :channels].astype(BF16).astype(F32)
    branch_x = projected[:, channels:].astype(BF16).astype(F32)
    convolved = history + tap[past:] * inner_x
    conv_round = convolved.astype(BF16)
    heads, head_width = wmap.shape[0], wmap.shape[1]

    def by_head(maps):
        return jnp.concatenate(
            [
                mm(conv_round[:, h * head_width : (h + 1) * head_width], maps[h])
                for h in range(heads)
            ],
            axis=1,
        )

    write_gate = jax.nn.sigmoid(by_head(wmap))
    decay_gate = jax.nn.sigmoid(by_head(dmap))
    forget = 8.0 * decay_gate * rates
    bent = jnp.tanh(forget)
    state_next = (
        jnp.exp(-forget) * state
        + jnp.sqrt(2.0 * bent / (1.0 + bent)) * write_gate * convolved
    )
    mixed = (state_next * jax.nn.gelu(branch_x)).astype(BF16)
    part_out[me_t] = mm(mixed, oproj[...]).astype(BF16)
    each(tp - 1, lambda n: over_tp(part_out, out_ss, out_rs, me_t, tp_peer(n)).start())

    for row in range(rows):
        next_s[row] = state_next[row : row + 1]
        inner_s[row] = inner_x[row : row + 1]
    state_out[...] = next_s[me_e]
    conv_out[0] = jnp.concatenate([conv_all[me_e].astype(F32)[1:], inner_s[me_e]], axis=0).astype(
        BF16
    )
    c_egain.wait()
    c_ids.wait()
    c_scores.wait()
    c_bgate.wait()
    score = scores[...]
    share = score / jnp.sum(score, axis=1, keepdims=True)
    chosen = jnp.sum(jnp.where(ids[...] == me_e, share, 0.0), axis=1, keepdims=True)
    gain2 = egain[...].astype(F32).reshape(1, width)
    mixer = bgate[...].astype(F32).reshape(1, width)
    for copy in local[len(small) :]:
        copy.wait()

    each(tp - 1, lambda n: over_tp(part_out, out_ss, out_rs, tp_peer(n), tp_peer(n)).wait_recv())
    resid = (tok + jnp.sum(part_out[...].astype(F32), axis=0)).astype(BF16).astype(F32)
    scale2 = lax.rsqrt(jnp.mean(resid * resid, axis=-1, keepdims=True) + 1e-06)
    normed2 = (resid * scale2 * gain2).astype(BF16)
    dense = (silu(mm(normed2, sg_w[...])) * mm(normed2, su_w[...])).astype(BF16)
    hidden = (silu(mm(normed2, eg_w[...])) * mm(normed2, eu_w[...])).astype(BF16)
    blend = jax.nn.sigmoid(jnp.sum(normed2.astype(F32) * mixer, axis=-1, keepdims=True))

    def last(col, row, slot):
        return pltpu.make_async_remote_copy(
            src_ref=part_send.at[col, row],
            dst_ref=part_recv.at[slot],
            send_sem=last_ss.at[row * tp + col],
            recv_sem=last_rs.at[slot],
            device_id={"ep": row, "tp": col},
            device_id_type=MESH,
        )

    for step in range(tp):
        col = lax.rem(me_t + 1 + step, tp)
        at = pl.ds(pl.multiple_of(col * col_width, col_width), col_width)
        sums = (chosen * mm(hidden, ed_w[:, at]) + blend * mm(dense, sd_w[:, at])).astype(BF16)
        for row in range(rows):
            part_send[col, row] = sums[row : row + 1]
        count = ep - 1 if step == tp - 1 else ep
        each(count, lambda n: last(col, ep_peer(n), me_flat).start())
    part_recv[me_flat] = part_send[me_t, me_e]
    for row in range(rows):
        resid_s[row] = resid[row : row + 1]
    own = resid_s[me_e, :, pl.ds(pl.multiple_of(me_t * col_width, col_width), col_width)]

    def other(number):
        flat = lax.rem(me_flat + 1 + number, ep * tp)
        return flat // tp, lax.rem(flat, tp), flat

    def recv_last(number):
        row, col, flat = other(number)
        last(col, row, flat).wait_recv()

    def sent_last(number):
        row, col, flat = other(number)
        last(col, row, flat).wait_send()

    each(ep * tp - 1, recv_last)
    total = own + jnp.sum(part_recv[...].astype(F32), axis=0)
    result_out[...] = total.astype(BF16)

    sent_ep(tok_all, tok_ss, tok_rs)
    sent_ep(conv_all, conv_ss, conv_rs)
    sent_ep(state_all, state_ss, state_rs)
    sent_ep(part_in, in_ss, in_rs)
    each(tp - 1, lambda n: over_tp(part_out, out_ss, out_rs, me_t, tp_peer(n)).wait_send())
    each(ep * tp - 1, sent_last)


def on_device(ep, tp, *args):
    (
        tokens,
        conv_state,
        state_h,
        mixer_gain,
        expert_gain,
        input_proj,
        branch_proj,
        conv_taps,
        write_map,
        decay_map,
        decay_rate,
        output_proj,
        route_ids,
        route_scores,
        expert_gate,
        expert_up,
        expert_down,
        branch_gate,
        shared_gate,
        shared_up,
        shared_down,
    ) = args
    assert tokens.shape[0] == 1
    rows = ep
    width = tokens.shape[1]
    channels = state_h.shape[1]
    col_width = width // tp
    past = conv_state.shape[1]

    def like(array):
        return pltpu.VMEM(array.shape, array.dtype)

    def inner(array):
        return pltpu.VMEM(array.shape[1:], array.dtype)

    dma = pltpu.SemaphoreType.DMA
    scratch = [
        pltpu.VMEM((rows, 1, width), BF16),
        pltpu.VMEM((rows, past, channels), BF16),
        pltpu.VMEM((rows, 1, channels), F32),
        like(mixer_gain),
        like(expert_gain),
        like(input_proj),
        like(branch_proj),
        like(conv_taps),
        like(write_map),
        like(decay_map),
        like(decay_rate),
        like(output_proj),
        like(route_ids),
        like(route_scores),
        inner(expert_gate),
        inner(expert_up),
        inner(expert_down),
        like(branch_gate),
        like(shared_gate),
        like(shared_up),
        like(shared_down),
        pltpu.VMEM((rows, width), F32),
        pltpu.VMEM((ep, rows, 2 * channels), BF16),
        pltpu.VMEM((tp, rows, width), BF16),
        pltpu.VMEM((tp, rows, 1, col_width), BF16),
        pltpu.VMEM((ep * tp, 1, col_width), BF16),
        pltpu.VMEM((rows, 1, width), F32),
        pltpu.VMEM((rows, 1, channels), F32),
        pltpu.VMEM((rows, 1, channels), F32),
        dma((len(args),)),
    ]
    scratch += [dma((ep,))] * 8 + [dma((tp,))] * 2 + [dma((ep * tp,))] * 2
    return pl.pallas_call(
        functools.partial(layer_kernel, ep, tp),
        out_shape=(
            jax.ShapeDtypeStruct((1, col_width), BF16),
            jax.ShapeDtypeStruct((1, channels), F32),
            jax.ShapeDtypeStruct((1, past, channels), BF16),
        ),
        in_specs=[pl.BlockSpec(memory_space=pl.ANY)] * len(args),
        out_specs=[pl.BlockSpec(memory_space=pltpu.VMEM)] * 3,
        scratch_shapes=scratch,
        compiler_params=pltpu.CompilerParams(
            collective_id=0, has_side_effects=True, vmem_limit_bytes=60 * 1024 * 1024
        ),
    )(*args)


def solution(mesh):
    placed = (
        P(("grp", "ep"), None),
        P(("grp", "ep"), None, "tp"),
        P(("grp", "ep"), "tp"),
        P(),
        P(),
        P("ep", "tp"),
        P("ep", "tp"),
        P(None, "tp"),
        P("tp", None, None),
        P("tp", None, None),
        P("tp"),
        P("tp", None),
        P("grp", None),
        P("grp", None),
        P("ep", None, "tp"),
        P("ep", None, "tp"),
        P("ep", "tp", None),
        P(),
        P(None, ("ep", "tp")),
        P(None, ("ep", "tp")),
        P(("ep", "tp"), None),
    )
    return jax.shard_map(
        functools.partial(on_device, mesh.shape["ep"], mesh.shape["tp"]),
        mesh=mesh,
        in_specs=placed,
        out_specs=(P(("grp", "ep"), "tp"), P(("grp", "ep"), "tp"), P(("grp", "ep"), None, "tp")),
        check_vma=False,
    )
```

time: 125 us -> 30.4 us (0.24)
  blocking collectives: 43.1 us -> 0 us
  Pallas kernels: 0 us -> 23.1 us
  waiting for transfers between devices: 22.8 us -> 0 us
  matrix products: 17.2 us -> 0 us
  between operations: 15.5 us -> 0.64 us
  other arithmetic: 11.8 us -> 0 us
  starting transfers between devices: 6.35 us -> 0 us
    unnamed x2 -> x0, blocking collectives: 24.2 us -> none
    pallas_call x0 -> x1, Pallas kernels: none -> 23.1 us  [on_device(): pl.pallas_call(functools.partial(layer_kernel, ep, tp), out_shape=(jax.Sh...]
    unnamed x2 -> x0, waiting for transfers between devices: 22.8 us -> none
    dot_general x13 -> x0, matrix products: 17.2 us -> none  [the longest x1 4.7 us: on_device(): jnp.dot(dense_hidden, shared_down, preferred_element_type=jnp.float32)]
    all_gather x1 -> x0, blocking collectives: 13.1 us -> none  [on_device(): gathered = lax.all_gather(normed2, 'ep', axis=0, tiled=True)]
    all_to_all x1 -> x0, starting transfers between devices: 6.35 us -> none  [on_device(): lax.all_to_all(normed, 'ep', split_axis=1, concat_axis=0, tiled=True)]
    psum x1 -> x0, blocking collectives: 5.74 us -> none  [on_device(): lax.psum(jnp.dot(mixed, output_proj, preferred_element_type=jnp.float32),...]
    reduce_sum x5 -> x0, other arithmetic: 4.08 us -> none  [the longest x2 2.64 us: rms_norm(): jnp.mean(values * values, axis=-1, keepdims=True) + 1e-06]
  transfers between devices with their start and end apart: 2 -> 0, of which waited for: 1 -> 0; matrix products, arithmetic and copies ran while one was open for 5% -> 0% of each run, Pallas kernels for 0% -> 0%
where the time goes in v1:
time: 30.4 us; the launch traced here: 30.2 us
  Pallas kernels  23.1 us (76%)
  local copies, waits for them, and re-layouts  6.39 us (21%)
  between operations  0.64 us (2%)
    pallas_call x1, Pallas kernels, on_device(): pl.pallas_call(functools.partial(layer_kernel, ep, tp), out_shape=(jax.Sh...  23.1 us
    unnamed x5, local copies, waits for them, and re-layouts  6.39 us

profile of v1, /device:TPU:0, one launch (start us, length us, event | category | flops | bytes accessed | tf_op | source)
XLA Modules:
  0.0 30.2 jit_solution(17714527606303526658)
XLA Ops:
  0.6 1.3 %copy.24.route_ids = s32[4,2]{1,0:T(4,128)} copy(s32[4,2]{0,1:T(2,128)} %param.33) | data formatting | bytes 64 | tf_op args[12]
  2.0 1.3 %copy.25.route_scores = f32[4,2]{1,0:T(4,128)} copy(f32[4,2]{0,1:T(2,128)} %param.34) | data formatting | bytes 64 | tf_op args[13]
  3.3 23.1 %shard_map.220 = (bf16[1,512]{1,0:T(2,128)(2,1)}, f32[1,256]{1,0:T(1,128)}, bf16[1,3,256]{2,1,0:T(4,128)(2,1)}) custom-call(bf16[1,2048]{1,0:T(2,128)(2,1)} %tokens.1, bf16[1,3,256]{2,1,0:T(4,128)(2,1)} %conv_state.1, f32[1,256]{1,0:T(1,128)} %state_h.1, bf16[2048]{0:T(1024)(128)(2,1)} %mixer_gain.1, bf16[2048]{0:T(1024)(128)(2,1)} %expert_gain.1, ...), custom_call_target="tpu_custom_call" | custom-call | tf_op jit(solution)/shard_map/pallas_call | solution.py:439
  26.4 1.3 %copy.29 = bf16[1,512]{1,0:T(2,128)(2,1)} copy(bf16[1,512]{1,0:T(2,128)(2,1)} %get-tuple-element.6) | data formatting | bytes 2048
  27.7 1.2 %copy.30 = f32[1,256]{1,0:T(1,128)} copy(f32[1,256]{1,0:T(1,128)} %get-tuple-element.7) | data formatting | bytes 2048
  28.9 1.2 %copy.31 = bf16[1,3,256]{2,1,0:T(4,128)(2,1)} copy(bf16[1,3,256]{2,1,0:T(4,128)(2,1)} %get-tuple-element.8) | data formatting | bytes 3072

commit v2 on v1

--- a/solution.py
+++ b/solution.py
@@ -303,8 +303,13 @@
     c_scores.wait()
     c_bgate.wait()
     score = scores[...]
-    share = score / jnp.sum(score, axis=1, keepdims=True)
-    chosen = jnp.sum(jnp.where(ids[...] == me_e, share, 0.0), axis=1, keepdims=True)
+    share = score / jnp.sum(score, axis=0, keepdims=True)
+    chosen = jnp.sum(jnp.where(ids[...] == me_e, share, 0.0), axis=0, keepdims=True)
+    square = (rows, rows)
+    diagonal = lax.broadcasted_iota(jnp.int32, square, 0) == lax.broadcasted_iota(
+        jnp.int32, square, 1
+    )
+    chosen = jnp.sum(jnp.where(diagonal, chosen, 0.0), axis=1, keepdims=True)
     gain2 = egain[...].astype(F32).reshape(1, width)
     mixer = bgate[...].astype(F32).reshape(1, width)
     for copy in local[len(small) :]:
@@ -363,6 +368,12 @@
     sent_ep(part_in, in_ss, in_rs)
     each(tp - 1, lambda n: over_tp(part_out, out_ss, out_rs, me_t, tp_peer(n)).wait_send())
     each(ep * tp - 1, sent_last)
+
+
+def hand_over(result, state, conv, result_out, state_out, conv_out):
+    result_out[...] = result[...]
+    state_out[...] = state[...]
+    conv_out[...] = conv[...]
 
 
 def on_device(ep, tp, *args):
@@ -390,6 +401,8 @@
         shared_down,
     ) = args
     assert tokens.shape[0] == 1
+    route_ids, route_scores = route_ids.T, route_scores.T
+    args = args[:12] + (route_ids, route_scores) + args[14:]
     rows = ep
     width = tokens.shape[1]
     channels = state_h.shape[1]
@@ -436,13 +449,14 @@
         dma((len(args),)),
     ]
     scratch += [dma((ep,))] * 8 + [dma((tp,))] * 2 + [dma((ep * tp,))] * 2
-    return pl.pallas_call(
+    shapes = (
+        jax.ShapeDtypeStruct((1, col_width), BF16),
+        jax.ShapeDtypeStruct((1, channels), F32),
+        jax.ShapeDtypeStruct((1, past, channels), BF16),
+    )
+    made = pl.pallas_call(
         functools.partial(layer_kernel, ep, tp),
-        out_shape=(
-            jax.ShapeDtypeStruct((1, col_width), BF16),
-            jax.ShapeDtypeStruct((1, channels), F32),
-            jax.ShapeDtypeStruct((1, past, channels), BF16),
-        ),
+        out_shape=shapes,
         in_specs=[pl.BlockSpec(memory_space=pl.ANY)] * len(args),
         out_specs=[pl.BlockSpec(memory_space=pltpu.VMEM)] * 3,
         scratch_shapes=scratch,
@@ -450,6 +464,12 @@
             collective_id=0, has_side_effects=True, vmem_limit_bytes=60 * 1024 * 1024
         ),
     )(*args)
+    return pl.pallas_call(
+        hand_over,
+        out_shape=shapes,
+        in_specs=[pl.BlockSpec(memory_space=pltpu.VMEM)] * 3,
+        out_specs=[pl.BlockSpec(memory_space=pltpu.VMEM)] * 3,
+    )(*made)
 
 
 def solution(mesh):

time: 30.4 us -> 25.3 us (0.83)
  local copies, waits for them, and re-layouts: 6.39 us -> 0 us
  Pallas kernels: 23.1 us -> 24.5 us
    unnamed x5 -> x0, local copies, waits for them, and re-layouts: 6.39 us -> none
    pallas_call x1 -> x2, Pallas kernels: 23.1 us -> 24.5 us  [the longest x1 23.2 us: on_device(): pl.pallas_call(functools.partial(layer_kernel, ep, tp), out_shape=shapes,...]
where the time goes in v2:
time: 25.3 us; the launch traced here: 25.1 us
  Pallas kernels  24.5 us (97%)
  between operations  0.65 us (3%)
    pallas_call x1, Pallas kernels, on_device(): pl.pallas_call(functools.partial(layer_kernel, ep, tp), out_shape=shapes,...  23.2 us
    pallas_call x1, Pallas kernels, on_device(): pl.pallas_call(hand_over, out_shape=shapes, in_specs=[pl.BlockSpec(memory...  1.27 us

profile of v2, /device:TPU:0, one launch (start us, length us, event | category | flops | bytes accessed | tf_op | source)
XLA Modules:
  0.0 25.1 jit_solution(11221113995328109670)
XLA Ops:
  0.6 23.2 %shard_map.220 = (bf16[1,512]{1,0:T(2,128)(2,1)}, f32[1,256]{1,0:T(1,128)}, bf16[1,3,256]{2,1,0:T(4,128)(2,1)}) custom-call(bf16[1,2048]{1,0:T(2,128)(2,1)} %tokens.1, bf16[1,3,256]{2,1,0:T(4,128)(2,1)} %conv_state.1, f32[1,256]{1,0:T(1,128)} %state_h.1, bf16[2048]{0:T(1024)(128)(2,1)} %mixer_gain.1, bf16[2048]{0:T(1024)(128)(2,1)} %expert_gain.1, ...), custom_call_target="tpu_custom_call" | custom-call | tf_op jit(solution)/shard_map/pallas_call | solution.py:457
  23.8 1.3 %shard_map.221 = (bf16[1,512]{1,0:T(2,128)(2,1)}, f32[1,256]{1,0:T(1,128)}, bf16[1,3,256]{2,1,0:T(4,128)(2,1)}) custom-call(bf16[1,512]{1,0:T(2,128)(2,1)} %get-tuple-element.6.result, f32[1,256]{1,0:T(1,128)} %get-tuple-element.7.state, bf16[1,3,256]{2,1,0:T(4,128)(2,1)} %get-tuple-element.8.conv), custom_call_target="tpu_custom_call" | custom-call | tf_op jit(solution)/shard_map/pallas_call | solution.py:467

commit v3 on v2

--- a/solution.py
+++ b/solution.py
@@ -169,17 +169,15 @@
 
     barrier = pltpu.get_barrier_semaphore()
 
-    def greet(number):
-        flat = lax.rem(me_flat + 1 + number, ep * tp)
-        pl.semaphore_signal(
-            barrier,
-            inc=1,
-            device_id={"ep": flat // tp, "tp": lax.rem(flat, tp)},
-            device_id_type=MESH,
-        )
-
-    each(ep * tp - 1, greet)
-    pl.semaphore_wait(barrier, ep * tp - 1)
+    def greet(peer):
+        pl.semaphore_signal(barrier, inc=1, device_id=peer, device_id_type=MESH)
+
+    each(ep - 1, lambda n: greet({"ep": lax.rem(me_e + 1 + n, ep)}))
+    each(tp - 1, lambda n: greet({"tp": lax.rem(me_t + 1 + n, tp)}))
+    c_mgain.wait()
+    gain1 = mgain[...].astype(F32).reshape(1, width)
+    norm_s[0:1] = gain1
+    pl.semaphore_wait(barrier, ep + tp - 2)
 
     def over_ep(buf, ssem, rsem, slot, peer):
         return pltpu.make_async_remote_copy(
@@ -225,24 +223,26 @@
     for copy in local[len(small) :]:
         copy.start()
 
-    c_mgain.wait()
     c_iproj.wait()
     c_bproj.wait()
     recv_ep(tok_all, tok_ss, tok_rs)
-    tok = jnp.concatenate([tok_all[row].astype(F32) for row in range(rows)], axis=0)
-    scale = lax.rsqrt(jnp.mean(tok * tok, axis=-1, keepdims=True) + 1e-06)
-    normed = tok * scale * mgain[...].astype(F32).reshape(1, width)
     if depth % 128 == 0:
-        norm_s[...] = normed
-        mine = norm_s[:, pl.ds(pl.multiple_of(me_e * depth, depth), depth)]
+        own_cols = pl.ds(pl.multiple_of(me_e * depth, depth), depth)
+        mine = jnp.concatenate(
+            [tok_all[row, :, own_cols].astype(F32) for row in range(rows)], axis=0
+        )
+        mine = mine * norm_s[0:1, own_cols]
     else:
-        mine = pltpu.roll(normed, lax.rem(width - me_e * depth, width), 1)[:, :depth]
+        mine = jnp.concatenate([tok_all[row].astype(F32) for row in range(rows)], axis=0) * gain1
+        mine = pltpu.roll(mine, lax.rem(width - me_e * depth, width), 1)[:, :depth]
     mine = mine.astype(BF16)
     part_in[me_e] = jnp.concatenate([mm(mine, iproj[...]), mm(mine, bproj[...])], axis=1).astype(
         BF16
     )
     send_ep(part_in, in_ss, in_rs)
 
+    tok = jnp.concatenate([tok_all[row].astype(F32) for row in range(rows)], axis=0)
+    scale = lax.rsqrt(jnp.mean(tok * tok, axis=-1, keepdims=True) + 1e-06)
     c_taps.wait()
     c_wmap.wait()
     c_dmap.wait()
@@ -263,7 +263,7 @@
     rates = rate[...].reshape(1, channels)
 
     recv_ep(part_in, in_ss, in_rs)
-    projected = jnp.sum(part_in[...].astype(F32), axis=0)
+    projected = jnp.sum(part_in[...].astype(F32), axis=0) * scale
     inner_x = projected[:, :channels].astype(BF16).astype(F32)
     branch_x = projected[:, channels:].astype(BF16).astype(F32)
     convolved = history + tap[past:] * inner_x
@@ -318,10 +318,11 @@
     each(tp - 1, lambda n: over_tp(part_out, out_ss, out_rs, tp_peer(n), tp_peer(n)).wait_recv())
     resid = (tok + jnp.sum(part_out[...].astype(F32), axis=0)).astype(BF16).astype(F32)
     scale2 = lax.rsqrt(jnp.mean(resid * resid, axis=-1, keepdims=True) + 1e-06)
-    normed2 = (resid * scale2 * gain2).astype(BF16)
-    dense = (silu(mm(normed2, sg_w[...])) * mm(normed2, su_w[...])).astype(BF16)
-    hidden = (silu(mm(normed2, eg_w[...])) * mm(normed2, eu_w[...])).astype(BF16)
-    blend = jax.nn.sigmoid(jnp.sum(normed2.astype(F32) * mixer, axis=-1, keepdims=True))
+    bare = resid * gain2
+    blend = jax.nn.sigmoid(jnp.sum(bare * mixer, axis=-1, keepdims=True) * scale2)
+    bare = bare.astype(BF16)
+    dense = (silu(mm(bare, sg_w[...]) * scale2) * (mm(bare, su_w[...]) * scale2)).astype(BF16)
+    hidden = (silu(mm(bare, eg_w[...]) * scale2) * (mm(bare, eu_w[...]) * scale2)).astype(BF16)
 
     def last(col, row, slot):
         return pltpu.make_async_remote_copy(
@@ -333,8 +334,15 @@
             device_id_type=MESH,
         )
 
-    for step in range(tp):
-        col = lax.rem(me_t + 1 + step, tp)
+    if tp % 2 == 0:
+        turn = me_t + 1 - 2 * lax.rem(me_t, 2)
+        order = [
+            lax.rem(base + 2 * pair, tp) for pair in range(1, tp // 2) for base in (me_t, turn)
+        ]
+        order += [turn, me_t]
+    else:
+        order = [lax.rem(me_t + 1 + step, tp) for step in range(tp)]
+    for step, col in enumerate(order):
         at = pl.ds(pl.multiple_of(col * col_width, col_width), col_width)
         sums = (chosen * mm(hidden, ed_w[:, at]) + blend * mm(dense, sd_w[:, at])).astype(BF16)
         for row in range(rows):
@@ -438,7 +446,7 @@
         like(shared_gate),
         like(shared_up),
         like(shared_down),
-        pltpu.VMEM((rows, width), F32),
+        pltpu.VMEM((8, width), F32),
         pltpu.VMEM((ep, rows, 2 * channels), BF16),
         pltpu.VMEM((tp, rows, width), BF16),
         pltpu.VMEM((tp, rows, 1, col_width), BF16),

time: 25.3 us -> 24.7 us (0.976)
  Pallas kernels: 24.5 us -> 23.9 us
    pallas_call x1, Pallas kernels: 23.2 us -> 22.6 us  [on_device(): pl.pallas_call(functools.partial(layer_kernel, ep, tp), out_shape=shapes,...]
where the time goes in v3:
time: 24.7 us; the launch traced here: 24.5 us
  Pallas kernels  23.9 us (97%)
  between operations  0.65 us (3%)
    pallas_call x1, Pallas kernels, on_device(): pl.pallas_call(functools.partial(layer_kernel, ep, tp), out_shape=shapes,...  22.6 us
    pallas_call x1, Pallas kernels, on_device(): pl.pallas_call(hand_over, out_shape=shapes, in_specs=[pl.BlockSpec(memory...  1.27 us

profile of v3, /device:TPU:0, one launch (start us, length us, event | category | flops | bytes accessed | tf_op | source)
XLA Modules:
  0.0 24.5 jit_solution(11477297954805850787)
XLA Ops:
  0.6 22.6 %shard_map.220 = (bf16[1,512]{1,0:T(2,128)(2,1)}, f32[1,256]{1,0:T(1,128)}, bf16[1,3,256]{2,1,0:T(4,128)(2,1)}) custom-call(bf16[1,2048]{1,0:T(2,128)(2,1)} %tokens.1, bf16[1,3,256]{2,1,0:T(4,128)(2,1)} %conv_state.1, f32[1,256]{1,0:T(1,128)} %state_h.1, bf16[2048]{0:T(1024)(128)(2,1)} %mixer_gain.1, bf16[2048]{0:T(1024)(128)(2,1)} %expert_gain.1, ...), custom_call_target="tpu_custom_call" | custom-call | tf_op jit(solution)/shard_map/pallas_call | solution.py:465
  23.3 1.3 %shard_map.221 = (bf16[1,512]{1,0:T(2,128)(2,1)}, f32[1,256]{1,0:T(1,128)}, bf16[1,3,256]{2,1,0:T(4,128)(2,1)}) custom-call(bf16[1,512]{1,0:T(2,128)(2,1)} %get-tuple-element.6.result, f32[1,256]{1,0:T(1,128)} %get-tuple-element.7.state, bf16[1,3,256]{2,1,0:T(4,128)(2,1)} %get-tuple-element.8.conv), custom_call_target="tpu_custom_call" | custom-call | tf_op jit(solution)/shard_map/pallas_call | solution.py:475

commit v4 on v3

--- a/solution.py
+++ b/solution.py
@@ -57,7 +57,8 @@
     shared_gate,
     shared_up,
     shared_down,
-    result_out,
+    part_recv,
+    own_out,
     state_out,
     conv_out,
     tok_all,
@@ -85,10 +86,11 @@
     part_in,
     part_out,
     part_send,
-    part_recv,
     resid_s,
     next_s,
     inner_s,
+    conv_s,
+    out_sem,
     local_sem,
     tok_ss,
     tok_rs,
@@ -294,10 +296,13 @@
     for row in range(rows):
         next_s[row] = state_next[row : row + 1]
         inner_s[row] = inner_x[row : row + 1]
-    state_out[...] = next_s[me_e]
-    conv_out[0] = jnp.concatenate([conv_all[me_e].astype(F32)[1:], inner_s[me_e]], axis=0).astype(
+    c_next = pltpu.make_async_copy(next_s.at[me_e], state_out, out_sem.at[0])
+    c_next.start()
+    conv_s[0] = jnp.concatenate([conv_all[me_e].astype(F32)[1:], inner_s[me_e]], axis=0).astype(
         BF16
     )
+    c_past = pltpu.make_async_copy(conv_s, conv_out, out_sem.at[1])
+    c_past.start()
     c_egain.wait()
     c_ids.wait()
     c_scores.wait()
@@ -349,10 +354,18 @@
             part_send[col, row] = sums[row : row + 1]
         count = ep - 1 if step == tp - 1 else ep
         each(count, lambda n: last(col, ep_peer(n), me_flat).start())
-    part_recv[me_flat] = part_send[me_t, me_e]
+    c_part = pltpu.make_async_copy(
+        part_send.at[me_t, me_e], part_recv.at[me_flat], out_sem.at[2]
+    )
+    c_part.start()
     for row in range(rows):
         resid_s[row] = resid[row : row + 1]
-    own = resid_s[me_e, :, pl.ds(pl.multiple_of(me_t * col_width, col_width), col_width)]
+    c_own = pltpu.make_async_copy(
+        resid_s.at[me_e, :, pl.ds(pl.multiple_of(me_t * col_width, col_width), col_width)],
+        own_out,
+        out_sem.at[3],
+    )
+    c_own.start()
 
     def other(number):
         flat = lax.rem(me_flat + 1 + number, ep * tp)
@@ -365,10 +378,6 @@
     def sent_last(number):
         row, col, flat = other(number)
         last(col, row, flat).wait_send()
-
-    each(ep * tp - 1, recv_last)
-    total = own + jnp.sum(part_recv[...].astype(F32), axis=0)
-    result_out[...] = total.astype(BF16)
 
     sent_ep(tok_all, tok_ss, tok_rs)
     sent_ep(conv_all, conv_ss, conv_rs)
@@ -376,10 +385,13 @@
     sent_ep(part_in, in_ss, in_rs)
     each(tp - 1, lambda n: over_tp(part_out, out_ss, out_rs, me_t, tp_peer(n)).wait_send())
     each(ep * tp - 1, sent_last)
-
-
-def hand_over(result, state, conv, result_out, state_out, conv_out):
-    result_out[...] = result[...]
+    for copy in (c_next, c_past, c_part, c_own):
+        copy.wait()
+    each(ep * tp - 1, recv_last)
+
+
+def hand_over(parts, own, state, conv, result_out, state_out, conv_out):
+    result_out[...] = (own[...] + jnp.sum(parts[...].astype(F32), axis=0)).astype(BF16)
     state_out[...] = state[...]
     conv_out[...] = conv[...]
 
@@ -450,10 +462,11 @@
         pltpu.VMEM((ep, rows, 2 * channels), BF16),
         pltpu.VMEM((tp, rows, width), BF16),
         pltpu.VMEM((tp, rows, 1, col_width), BF16),
-        pltpu.VMEM((ep * tp, 1, col_width), BF16),
         pltpu.VMEM((rows, 1, width), F32),
         pltpu.VMEM((rows, 1, channels), F32),
         pltpu.VMEM((rows, 1, channels), F32),
+        pltpu.VMEM((1, past, channels), BF16),
+        dma((4,)),
         dma((len(args),)),
     ]
     scratch += [dma((ep,))] * 8 + [dma((tp,))] * 2 + [dma((ep * tp,))] * 2
@@ -464,9 +477,13 @@
     )
     made = pl.pallas_call(
         functools.partial(layer_kernel, ep, tp),
-        out_shape=shapes,
+        out_shape=(
+            jax.ShapeDtypeStruct((ep * tp, 1, col_width), BF16),
+            jax.ShapeDtypeStruct((1, col_width), F32),
+        )
+        + shapes[1:],
         in_specs=[pl.BlockSpec(memory_space=pl.ANY)] * len(args),
-        out_specs=[pl.BlockSpec(memory_space=pltpu.VMEM)] * 3,
+        out_specs=[pl.BlockSpec(memory_space=pl.ANY)] * 4,
         scratch_shapes=scratch,
         compiler_params=pltpu.CompilerParams(
             collective_id=0, has_side_effects=True, vmem_limit_bytes=60 * 1024 * 1024
@@ -475,7 +492,7 @@
     return pl.pallas_call(
         hand_over,
         out_shape=shapes,
-        in_specs=[pl.BlockSpec(memory_space=pltpu.VMEM)] * 3,
+        in_specs=[pl.BlockSpec(memory_space=pltpu.VMEM)] * 4,
         out_specs=[pl.BlockSpec(memory_space=pltpu.VMEM)] * 3,
     )(*made)
 

time: 24.7 us -> 24.3 us (0.984)
  Pallas kernels: 23.9 us -> 23.4 us
    pallas_call x1, Pallas kernels: 22.6 us -> 22 us  [on_device(): pl.pallas_call(functools.partial(layer_kernel, ep, tp), out_shape=(jax.Sh...]
where the time goes in v4:
time: 24.3 us; the launch traced here: 24.1 us
  Pallas kernels  23.4 us (96%)
  between operations  0.65 us (3%)
    pallas_call x1, Pallas kernels, on_device(): pl.pallas_call(functools.partial(layer_kernel, ep, tp), out_shape=(jax.Sh...  22 us
    pallas_call x1, Pallas kernels, on_device(): pl.pallas_call(hand_over, out_shape=shapes, in_specs=[pl.BlockSpec(memory...  1.39 us

profile of v4, /device:TPU:0, one launch (start us, length us, event | category | flops | bytes accessed | tf_op | source)
XLA Modules:
  0.0 24.1 jit_solution(8136355210563836009)
XLA Ops:
  0.6 22.0 %shard_map.220 = (bf16[16,1,512]{2,1,0:T(2,128)(2,1)}, f32[1,512]{1,0:T(1,128)}, f32[1,256]{1,0:T(1,128)}, bf16[1,3,256]{2,1,0:T(4,128)(2,1)}) custom-call(bf16[1,2048]{1,0:T(2,128)(2,1)} %tokens.1, bf16[1,3,256]{2,1,0:T(4,128)(2,1)} %conv_state.1, f32[1,256]{1,0:T(1,128)} %state_h.1, bf16[2048]{0:T(1024)(128)(2,1)} %mixer_gain.1, ...), custom_call_target="tpu_custom_call" | custom-call | tf_op jit(solution)/shard_map/pallas_call | solution.py:478
  22.7 1.4 %shard_map.221 = (bf16[1,512]{1,0:T(2,128)(2,1)}, f32[1,256]{1,0:T(1,128)}, bf16[1,3,256]{2,1,0:T(4,128)(2,1)}) custom-call(bf16[16,1,512]{2,1,0:T(2,128)(2,1)} %get-tuple-element.7.parts, f32[1,512]{1,0:T(1,128)} %get-tuple-element.8.own, f32[1,256]{1,0:T(1,128)} %get-tuple-element.9.state, bf16[1,3,256]{2,1,0:T(4,128)(2,1)} %get-tuple-element.10.conv), custom_call_target="tpu_custom_call" | custom-call | tf_op jit(solution)/shard_map/pallas_call | solution.py:492

commit v5 on v4

--- a/solution.py
+++ b/solution.py
@@ -204,11 +204,14 @@
     def ep_peer(number):
         return lax.rem(me_e + 1 + number, ep)
 
+    def far_peer(number):
+        return lax.rem(me_e + 1 + (number + ep // 2 - 1) % (ep - 1), ep)
+
     def tp_peer(number):
         return lax.rem(me_t + 1 + number, tp)
 
     def send_ep(buf, ssem, rsem):
-        each(ep - 1, lambda n: over_ep(buf, ssem, rsem, me_e, ep_peer(n)).start())
+        each(ep - 1, lambda n: over_ep(buf, ssem, rsem, me_e, far_peer(n)).start())
 
     def recv_ep(buf, ssem, rsem):
         each(ep - 1, lambda n: over_ep(buf, ssem, rsem, ep_peer(n), ep_peer(n)).wait_recv())
@@ -352,8 +355,9 @@
         sums = (chosen * mm(hidden, ed_w[:, at]) + blend * mm(dense, sd_w[:, at])).astype(BF16)
         for row in range(rows):
             part_send[col, row] = sums[row : row + 1]
-        count = ep - 1 if step == tp - 1 else ep
-        each(count, lambda n: last(col, ep_peer(n), me_flat).start())
+        each(ep - 1, lambda n: last(col, far_peer(n), me_flat).start())
+        if step < tp - 1:
+            last(col, me_e, me_flat).start()
     c_part = pltpu.make_async_copy(
         part_send.at[me_t, me_e], part_recv.at[me_flat], out_sem.at[2]
     )

time: 24.3 us -> 24.4 us (level)
  no operation moved by 1% of the time
where the time goes in v5:
time: 24.4 us; the launch traced here: 24.2 us
  Pallas kernels  23.5 us (96%)
  between operations  0.65 us (3%)
    pallas_call x1, Pallas kernels, on_device(): pl.pallas_call(functools.partial(layer_kernel, ep, tp), out_shape=(jax.Sh...  22.1 us
    pallas_call x1, Pallas kernels, on_device(): pl.pallas_call(hand_over, out_shape=shapes, in_specs=[pl.BlockSpec(memory...  1.39 us

profile of v5, /device:TPU:0, one launch (start us, length us, event | category | flops | bytes accessed | tf_op | source)
XLA Modules:
  0.0 24.2 jit_solution(15963166556803978255)
XLA Ops:
  0.6 22.1 %shard_map.220 = (bf16[16,1,512]{2,1,0:T(2,128)(2,1)}, f32[1,512]{1,0:T(1,128)}, f32[1,256]{1,0:T(1,128)}, bf16[1,3,256]{2,1,0:T(4,128)(2,1)}) custom-call(bf16[1,2048]{1,0:T(2,128)(2,1)} %tokens.1, bf16[1,3,256]{2,1,0:T(4,128)(2,1)} %conv_state.1, f32[1,256]{1,0:T(1,128)} %state_h.1, bf16[2048]{0:T(1024)(128)(2,1)} %mixer_gain.1, ...), custom_call_target="tpu_custom_call" | custom-call | tf_op jit(solution)/shard_map/pallas_call | solution.py:482
  22.8 1.4 %shard_map.221 = (bf16[1,512]{1,0:T(2,128)(2,1)}, f32[1,256]{1,0:T(1,128)}, bf16[1,3,256]{2,1,0:T(4,128)(2,1)}) custom-call(bf16[16,1,512]{2,1,0:T(2,128)(2,1)} %get-tuple-element.7.parts, f32[1,512]{1,0:T(1,128)} %get-tuple-element.8.own, f32[1,256]{1,0:T(1,128)} %get-tuple-element.9.state, bf16[1,3,256]{2,1,0:T(4,128)(2,1)} %get-tuple-element.10.conv), custom_call_target="tpu_custom_call" | custom-call | tf_op jit(solution)/shard_map/pallas_call | solution.py:496
